TPU v7x, 32 devices: a whole 2x2x4 slice. The times are simulated.
32 devices in a mesh: sp: 4 (over z), fs: 4 (over y, x), tp: 2 (over core).
Axes of the slice: x: 2, y: 2, z: 4, core: 2. Of those that a mesh axis runs over, the one named last changes fastest.
Arguments:
- tokens: bfloat16 [4, 512, 4096], P('fs', 'sp'), may hold values from -6 to 6
- norm_gain: float32 [4096], replicated, may hold values from 0.1 to 1.9
- pool_proj: bfloat16 [4096, 1024], P(('sp', 'fs'), 'tp'), may hold values from -0.09375 to 0.09375
- query_proj: bfloat16 [4096, 1024], P(('sp', 'fs'), 'tp'), may hold values from -0.09375 to 0.09375
- key_proj: bfloat16 [4096, 1024], P(('sp', 'fs'), 'tp'), may hold values from -0.09375 to 0.09375
- value_proj: bfloat16 [4096, 1024], P(('sp', 'fs'), 'tp'), may hold values from -0.09375 to 0.09375
- pool_map: bfloat16 [4, 256, 256], replicated, may hold values from -0.375 to 0.375
- pool_scale: float32 [1024], replicated, may hold values from 0.1 to 1.9
- decay_rate: float32 [4], P('tp'), may hold values from 2e-05 to 0.034
- start_state: float32 [4, 4, 256, 256], P('fs', 'tp', 'sp'), may hold values from -96 to 96
- pool_back: bfloat16 [1024, 4096], P('tp', ('sp', 'fs')), may hold values from -0.125 to 0.125
- retention_back: bfloat16 [1024, 4096], P('tp', ('sp', 'fs')), may hold values from -0.125 to 0.125
Outputs:
- mixed: bfloat16 [4, 512, 4096], P('fs', ('sp', 'tp'))
All inputs are finite; a program needn't handle non-finite values.
Results may differ from a plain program's by a relative error of at most 0.014.
Values may be sent and summed in bfloat16 or wider, within the bound.
A program may use at most 128 MiB of HBM per device.

v0:
```python
import jax
import jax.numpy as jnp
from jax import lax
from jax.sharding import PartitionSpec as P

GROUPS = 4
BLOCK = 128
HALO = 16
eps = 1e-06
rope_base = 10000.0
highest_precision = lax.Precision.HIGHEST
window_list = (2, 4, 8, 16)


def shortened(x):
    return jax.tree.map(lambda a: a.astype(jnp.bfloat16) if a.dtype == jnp.float32 else a, x)


def shifted(x, axis, by):
    devices = lax.axis_size(axis)
    pairs = [(i, i + by) for i in range(devices) if 0 <= i + by < devices]
    return lax.ppermute(x, axis, pairs)


def carried_in(value, axis, join, neutral):
    count, mine = (lax.axis_size(axis), lax.axis_index(axis))
    pieces = jax.tree.map(lambda part: lax.all_gather(part, axis), value)
    running = jax.tree.map(
        lambda part, zero: jnp.full_like(part, 0) + jnp.asarray(zero, part.dtype), value, neutral
    )

    def turn(position, running):
        longer = join(running, jax.tree.map(lambda part: part[position], pieces))
        return jax.tree.map(lambda new, old: jnp.where(position < mine, new, old), longer, running)

    return lax.fori_loop(0, count - 1, turn, running)


def rotate(values, positions):
    half_dim = values.shape[-1] // 2
    inv_freq = 1.0 / rope_base ** jnp.linspace(0.0, 1.0, half_dim, dtype=jnp.float32)
    angles = positions.astype(jnp.float32)[:, None] * inv_freq[None, :]
    cosine = jnp.cos(angles)[:, None, :]
    sine = jnp.sin(angles)[:, None, :]
    first_half = values[..., :half_dim]
    second_half = values[..., half_dim:]
    return jnp.concatenate(
        [first_half * cosine - second_half * sine, first_half * sine + second_half * cosine],
        axis=-1,
    )


def trailing_sums(extended, length):
    begin = extended.shape[0] - length
    running = extended[begin:]
    results = []
    for behind in range(1, 16):
        running = running + extended[begin - behind : begin - behind + length]
        if behind + 1 in window_list:
            results.append(running)
    return results


def reshape_blocks(array):
    return array.reshape((array.shape[0] // BLOCK, BLOCK) + array.shape[1:])


def block_retention(queries, keys_in, values_in, decay_rate, initial):
    length, head_count, head_dim = queries.shape
    within = jnp.arange(BLOCK, dtype=jnp.float32)
    distance = within[:, None] - within[None, :]
    decay_mask = jnp.where(
        distance[None] >= 0,
        jnp.exp(-jnp.maximum(distance, 0.0)[None] * decay_rate[:, None, None]),
        0.0,
    )
    query_decay_factor = jnp.exp(-(within + 1.0)[:, None] * decay_rate[None, :])
    key_decay_factor = jnp.exp(-(BLOCK - 1.0 - within)[:, None] * decay_rate[None, :])
    block_decay_factor = jnp.exp(-BLOCK * decay_rate)

    def advance(state_carry, inputs):
        block_queries, block_keys, block_values = inputs
        scores = (
            jnp.einsum("ihk,jhk->hij", block_queries, block_keys, precision=highest_precision)
            * decay_mask
        )
        inside = jnp.einsum("hij,jhv->ihv", scores, block_values, precision=highest_precision)
        across_blocks = jnp.einsum(
            "bzy,zyx->bzx",
            block_queries * query_decay_factor[:, :, None],
            state_carry,
            precision=highest_precision,
        )
        state_carry = state_carry * block_decay_factor[:, None, None] + jnp.einsum(
            "flm,fld->lmd",
            block_keys * key_decay_factor[:, :, None],
            block_values,
            precision=highest_precision,
        )
        return (state_carry, inside + across_blocks)

    final_state, outputs = lax.scan(
        advance,
        initial,
        (reshape_blocks(queries), reshape_blocks(keys_in), reshape_blocks(values_in)),
    )
    return (outputs.reshape(length, head_count, values_in.shape[-1]), final_state)


def combine_states(earlier, latter):
    return (earlier[0] * latter[0], latter[0][:, None, None] * earlier[1] + latter[1])


def on_device(
    tokens,
    norm_gain,
    pool_proj,
    query_proj,
    key_proj,
    value_proj,
    pool_map,
    pool_scale,
    decay_rate,
    start_state,
    pool_back,
    retention_back,
):
    sequence = tokens[0]
    length = sequence.shape[0]
    tp_index = lax.axis_index("tp")
    sp_index = lax.axis_index("sp")
    tp_count = lax.axis_size("tp")
    floats = sequence.astype(jnp.float32)
    normed = (
        floats * lax.rsqrt(jnp.mean(floats * floats, axis=-1, keepdims=True) + eps) * norm_gain
    ).astype(jnp.bfloat16)
    group_normed = lax.all_gather(normed, "fs", axis=0, tiled=True)
    quarters = (
        lax.all_to_all(pool_proj, "fs", split_axis=1, concat_axis=0, tiled=True),
        lax.all_to_all(query_proj, "fs", split_axis=1, concat_axis=0, tiled=True),
        lax.all_to_all(key_proj, "fs", split_axis=1, concat_axis=0, tiled=True),
        lax.all_to_all(value_proj, "fs", split_axis=1, concat_axis=0, tiled=True),
    )
    pieces = (
        lax.all_gather(quarters[0], "sp", axis=0, tiled=True),
        lax.all_gather(quarters[1], "sp", axis=0, tiled=True),
        lax.all_gather(quarters[2], "sp", axis=0, tiled=True),
        lax.all_gather(quarters[3], "sp", axis=0, tiled=True),
    )
    partial_cols = tuple(
        (jnp.dot(group_normed, piece_w, preferred_element_type=jnp.float32) for piece_w in pieces)
    )
    rounded = tuple((result.astype(jnp.bfloat16) for result in partial_cols))
    pool_in, query_bf, key_bf, value_bf = jax.tree.map(
        lambda part, own: part.astype(own.dtype),
        lax.all_to_all(shortened(rounded), "fs", split_axis=0, concat_axis=1, tiled=True),
        rounded,
    )
    positions = jnp.arange(length, dtype=jnp.int32) + sp_index * length
    before = shifted(pool_in[length - HALO :], "sp", 1)
    extended = jnp.concatenate([before, pool_in], axis=0).astype(jnp.float32)
    stacked = jnp.stack(trailing_sums(extended, length))
    local_groups = GROUPS // tp_count
    channels = pool_in.shape[1]
    group_dim = channels // local_groups
    group_maps = lax.dynamic_slice_in_dim(pool_map, tp_index * local_groups, local_groups, 0)
    scales = lax.dynamic_slice_in_dim(pool_scale, tp_index * channels, channels, 0)
    windows = jnp.array(window_list, dtype=jnp.int32)
    pieces = []
    for group_idx in range(local_groups):
        chosen_group = tp_index * local_groups + group_idx
        lower = group_idx * group_dim
        chosen = lax.dynamic_index_in_dim(stacked, chosen_group, 0, keepdims=False)[
            :, lower : lower + group_dim
        ]
        counts = jnp.minimum(windows[chosen_group], positions + 1).astype(jnp.float32)
        inputs = extended[HALO:, lower : lower + group_dim]
        differ = (chosen / counts[:, None] - inputs).astype(jnp.bfloat16)
        pieces.append(jnp.dot(differ, group_maps[group_idx], preferred_element_type=jnp.float32))
    pool_out = (jnp.concatenate(pieces, axis=1) * scales).astype(jnp.bfloat16)
    head_count = decay_rate.shape[0]
    head_dim = query_bf.shape[1] // head_count
    queries = rotate(query_bf.astype(jnp.float32).reshape(length, head_count, head_dim), positions)
    keys_in = rotate(
        key_bf.astype(jnp.float32).reshape(length, head_count, head_dim), positions
    ) * head_dim ** (-0.5)
    values_in = value_bf.astype(jnp.float32).reshape(length, head_count, head_dim)
    zeros_state = jnp.zeros((head_count, head_dim, head_dim), jnp.float32)
    local_output, local_state = block_retention(
        queries, keys_in, values_in, decay_rate, zeros_state
    )
    span_decay = jnp.exp(-decay_rate * length)
    whole_start = lax.all_gather(start_state, "sp", axis=2, tiled=True)[0]
    span_factor, carried_over = carried_in(
        (span_decay, local_state), "sp", combine_states, (jnp.ones_like(span_decay), zeros_state)
    )
    offset_float = (sp_index * length).astype(jnp.float32)
    carried_over = carried_over + jnp.exp(-decay_rate * offset_float)[:, None, None] * whole_start
    steps_in = jnp.arange(length, dtype=jnp.float32) + 1.0
    query_rows_scaled = queries * jnp.exp(-steps_in[:, None] * decay_rate[None, :])[:, :, None]
    retained_output = local_output + jnp.einsum(
        "lpi,pib->lpb", query_rows_scaled, carried_over, precision=highest_precision
    )
    retained_output = retained_output * lax.rsqrt(
        jnp.mean(retained_output * retained_output, axis=-1, keepdims=True) + eps
    )
    ret_out = retained_output.reshape(length, head_count * head_dim).astype(jnp.bfloat16)
    pool_cols, retention_cols = (
        lax.all_gather(pool_back, ("sp", "fs"), axis=1, tiled=True),
        lax.all_gather(retention_back, ("sp", "fs"), axis=1, tiled=True),
    )
    weight_local = jnp.concatenate([pool_cols, retention_cols], axis=0)
    joined = jnp.concatenate([pool_out, ret_out], axis=1)
    mixed = lax.psum_scatter(
        jnp.dot(joined, weight_local, preferred_element_type=jnp.float32).astype(jnp.bfloat16),
        "tp",
        scatter_dimension=0,
        tiled=True,
    )
    return mixed[None]


def solution(mesh):
    placed = (
        P("fs", "sp", None),
        P(),
        P(("sp", "fs"), "tp"),
        P(("sp", "fs"), "tp"),
        P(("sp", "fs"), "tp"),
        P(("sp", "fs"), "tp"),
        P(),
        P(),
        P("tp"),
        P("fs", "tp", "sp", None),
        P("tp", ("sp", "fs")),
        P("tp", ("sp", "fs")),
    )
    return jax.shard_map(
        on_device,
        mesh=mesh,
        in_specs=placed,
        out_specs=P("fs", ("sp", "tp"), None),
        check_vma=False,
    )
```

profile of v0, /device:TPU:0, one launch (start us, length us, event | category | flops | bytes accessed | tf_op | source)
XLA Modules:
  0.0 432.0 jit_solution(100196734017617633)
XLA Ops:
  6.5 1.2 copy.58
  7.7 10.7 %all_to_all.137 = bf16[256,4,128]{0,2,1:T(8,128)(2,1)S(1)} all-to-all(bf16[256,4,128]{0,2,1:T(8,128)(2,1)S(1)} %bitcast.100), channel_id=1, replica_groups=mesh['sp'=4,'fs'=4,'tp'=2] {'fs'}, dimensions={1} | all-to-all | bytes 524288 | tf_op jit(solution)/shard_map/all_to_all | solution.py:140
  18.4 0.9 copy.59
  19.4 1.5 fusion.8
  20.9 2.6 fusion.10
  23.6 0.1 copy.63
  23.7 8.1 %all_to_all.138 = bf16[256,4,128]{0,2,1:T(8,128)(2,1)S(1)} all-to-all(bf16[256,4,128]{0,2,1:T(8,128)(2,1)S(1)} %bitcast.101), channel_id=1, replica_groups=mesh['sp'=4,'fs'=4,'tp'=2] {'fs'}, dimensions={1} | all-to-all | bytes 524288 | tf_op jit(solution)/shard_map/all_to_all | solution.py:141
  31.9 0.8 copy.64
  32.8 0.1 copy.55
  32.9 8.1 %all_to_all.139 = bf16[256,4,128]{0,2,1:T(8,128)(2,1)S(1)} all-to-all(bf16[256,4,128]{0,2,1:T(8,128)(2,1)S(1)} %bitcast.102), channel_id=1, replica_groups=mesh['sp'=4,'fs'=4,'tp'=2] {'fs'}, dimensions={1} | all-to-all | bytes 524288 | tf_op jit(solution)/shard_map/all_to_all | solution.py:142
  41.0 0.8 copy.56
  41.9 0.8 copy.50
  42.8 3.4 all-to-all-start
  46.2 0.6 dynamic-slice.2
  47.6 0.3 multiply_cosine_fusion
  47.9 0.1 multiply_exponential_fusion.1
  48.0 3.5 all-to-all-done
  51.5 0.9 copy.51
  52.4 48.6 %all-gather.11.cloned.1.call-done = bf16[512,4096]{1,0:T(8,128)(2,1)} async-done(((bf16[128,4096]{1,0:T(8,128)(2,1)}), bf16[512,4096]{1,0:T(8,128)(2,1)}) %all-gather.11.cloned.1.call-update) | async-done | bytes 4194320 | tf_op jit(solution)/shard_map/all_gather | solution.py:137
  101.0 3.7 convolution_convert_fusion.1
  104.7 0.8 copy.60
  105.5 3.3 all-to-all-start.5
  108.8 21.8 %all-gather.19.cloned.1.call-done = bf16[4096,128]{1,0:T(8,128)(2,1)} async-done(((bf16[1024,128]{1,0:T(8,128)(2,1)}), bf16[4096,128]{1,0:T(8,128)(2,1)}) %all-gather.19.cloned.1.call-update) | async-done | bytes 1048592 | tf_op jit(solution)/shard_map/all_gather | solution.py:147
  130.6 3.7 convolution_convert_fusion
  134.3 0.8 copy.65
  135.1 3.7 all-to-all-start.7
  138.7 20.7 %all-gather.15.cloned.1.call-done = bf16[4096,128]{1,0:T(8,128)(2,1)} async-done(((bf16[1024,128]{1,0:T(8,128)(2,1)}), bf16[4096,128]{1,0:T(8,128)(2,1)}) %all-gather.15.cloned.1.call-update) | async-done | bytes 1048592 | tf_op jit(solution)/shard_map/all_gather | solution.py:148
  159.4 4.4 %convolution_convert_fusion.2 = bf16[512,128]{1,0:T(8,128)(2,1)} fusion(bf16[512,4096]{1,0:T(8,128)(2,1)} %all-gather.11.cloned.1.call-done, bf16[4096,128]{1,0:T(8,128)(2,1)} %all-gather.15.cloned.1.call-done), kind=kOutput, calls=%fused_computation.19 | convolution fusion | flops 536936448 | bytes 5373952 | tf_op jit(solution)/shard_map/dot_general | solution.py:151
  163.8 3.8 all-to-all-start.3
  168.1 4.5 %all-to-all-done.3 = bf16[4,128,128]{2,1,0:T(8,128)(2,1)S(1)} async-done(((bf16[4,128,128]{2,1,0:T(8,128)(2,1)}), bf16[4,128,128]{2,1,0:T(8,128)(2,1)S(1)}, u32[]{:S(2)}, u32[]{:S(2)}) %all-to-all-start.3) | async-done | bytes 131104 | tf_op jit(solution)/shard_map/all_to_all | solution.py:156
  172.7 0.1 copy.57
  172.9 1.3 convolution_add_fusion
  174.2 0.7 all-gather.21.cloned.1.call-update
  175.0 0.7 all-gather.23.cloned.1.call-update
  175.7 10.7 %all-reduce = f32[8]{0:T(128)S(1)} all-reduce(f32[8]{0:T(128)S(1)} %get-tuple-element.181), channel_id=2, replica_groups=mesh['sp'=4,'fs'=4,'tp'=2] {'sp'}, use_global_device_ids=true, to_apply=%add | all-reduce | flops 8 | bytes 64
  186.5 0.6 fusion.53
  187.2 14.7 %all_gather.45 = f32[1,2,256,256]{3,2,1,0:T(8,128)S(1)} all-gather(f32[1,2,64,256]{3,2,1,0:T(8,128)S(1)} %copy-done.4), channel_id=1, replica_groups=mesh['sp'=4,'fs'=4,'tp'=2] {'sp'}, dimensions={2}, use_global_device_ids=true | all-gather | bytes 655360 | tf_op jit(solution)/shard_map/all_gather | solution.py:193
  201.9 3.7 convolution_convert_fusion.3
  205.6 0.8 copy.52
  206.4 3.3 all-to-all-start.1
  209.8 1.3 minimum_convert_fusion
  211.1 3.7 all-to-all-done.1
  214.7 0.1 slice.112
  214.9 3.1 collective-permute-start
  218.0 0.4 convolution_multiply_fusion
  218.4 0.3 fusion.54
  218.7 0.7 convolution_add_fusion.2
  219.4 0.2 collective-permute-done
  219.6 0.1 copy.54
  219.7 0.1 maximum_convert_fusion
  219.8 1.1 fusion.14
  221.1 0.3 fusion.27
  221.4 0.3 fusion.25
  221.7 14.9 %all-gather.25.cloned.1.call-done = f32[8,256,256]{2,1,0:T(8,128)} async-done(((f32[2,256,256]{2,1,0:T(8,128)}), f32[8,256,256]{2,1,0:T(8,128)}) %all-gather.25.cloned.1.call-update) | async-done | bytes 2097168 | tf_op jit(solution)/shard_map/all_gather | solution.py:27
  236.6 3.6 while.9
  236.6 1.2 fusion.67
  237.8 1.2 fusion.67
  239.0 1.2 fusion.67
  240.2 1.2 multiply_reduce_fusion
  241.4 0.1 copy.76
  241.5 83.7 %all-gather.21.cloned.1.call-done = bf16[512,4096]{1,0:T(8,128)(2,1)} async-done(((bf16[512,256]{1,0:T(8,128)(2,1)}), bf16[512,4096]{1,0:T(8,128)(2,1)}) %all-gather.21.cloned.1.call-update) | async-done | bytes 4194320 | tf_op jit(solution)/shard_map/all_gather | solution.py:209
  325.2 87.7 %all-gather.23.cloned.1.call-done = bf16[512,4096]{1,0:T(8,128)(2,1)} async-done(((bf16[512,256]{1,0:T(8,128)(2,1)}), bf16[512,4096]{1,0:T(8,128)(2,1)}) %all-gather.23.cloned.1.call-update) | async-done | bytes 4194320 | tf_op jit(solution)/shard_map/all_gather | solution.py:210
  412.9 5.8 %fusion.5 = bf16[128,4096]{1,0:T(8,128)(2,1)} fusion(bf16[512,4096]{1,0:T(8,128)(2,1)} %all-gather.23.cloned.1.call-done, bf16[512,4096]{1,0:T(8,128)(2,1)} %all-gather.21.cloned.1.call-done, bf16[128,512]{1,0:T(8,128)(2,1)S(1)} %copy.76, bf16[128,512]{1,0:T(8,128)(2,1)S(1)} %fusion.15), kind=kOutput, calls=%fused_computation.7 | convolution fusion | flops 1091567616 | bytes 9699328 | tf_op jit(solution)/shard_map/dot_general | solution.py:215
  418.8 6.7 %reduce-scatter.2.cloned.1.call-done = bf16[64,4096]{1,0:T(8,128)(2,1)} async-done(((bf16[128,4096]{1,0:T(8,128)(2,1)}), bf16[64,4096]{1,0:T(8,128)(2,1)}) %reduce-scatter.2.cloned.1.call-update) | async-done | bytes 524304 | tf_op jit(solution)/shard_map/reduce_scatter | solution.py:214
  (68 shorter events, 1.7 us)
Async XLA Ops:
  6.5 214.6 %copy-start = (bf16[4,256,256]{2,1,0:T(8,128)(2,1)S(1)}, bf16[4,256,256]{2,1,0:T(8,128)(2,1)}, u32[]{:S(2)}) copy-start(bf16[4,256,256]{2,1,0:T(8,128)(2,1)} %param.23) | copy-start | bytes 1572868
  6.5 17.1 %copy-start.1 = (bf16[256,512]{1,0:T(8,128)(2,1)S(1)}, bf16[256,512]{1,0:T(8,128)(2,1)}, u32[]{:S(2)}) copy-start(bf16[256,512]{1,0:T(8,128)(2,1)} %param.21) | copy-start | bytes 786436
  6.5 26.2 %copy-start.2 = (bf16[256,512]{1,0:T(8,128)(2,1)S(1)}, bf16[256,512]{1,0:T(8,128)(2,1)}, u32[]{:S(2)}) copy-start(bf16[256,512]{1,0:T(8,128)(2,1)} %param.22) | copy-start | bytes 786436
  6.5 45.9 %all-gather.17.cloned.1.call-start = ((), (), s32[]{:S(2)}) async-start(), calls=%async_computation.12 | async-start | bytes 1310720 | tf_op jit(solution)/shard_map/all_gather | solution.py:146
  19.3 22.6 %copy-start.3 = (bf16[256,512]{1,0:T(8,128)(2,1)S(1)}, bf16[256,512]{1,0:T(8,128)(2,1)}, u32[]{:S(2)}) copy-start(bf16[256,512]{1,0:T(8,128)(2,1)} %param.19) | copy-start | bytes 786436
  19.3 81.7 %all-gather.11.cloned.1.call-start = ((), (), s32[]{:S(2)}) async-start(), calls=%async_computation.9 | async-start | bytes 5242880 | tf_op jit(solution)/shard_map/all_gather | solution.py:137
  20.9 25.3 %copy-start.8 = (u32[32]{0:T(128)S(1)}, u32[32]{0:T(128)}, u32[]{:S(2)}) copy-start(u32[32]{0:T(128)} %constant.104) | copy-start | bytes 388
  20.9 26.6 %copy-start.5 = (f32[2]{0:T(128)S(1)}, f32[2]{0:T(128)}, u32[]{:S(2)}) copy-start(f32[2]{0:T(128)} %param.25) | copy-start | bytes 28
  23.5 107.0 %all-gather.19.cloned.1.call-start = ((), (), s32[]{:S(2)}) async-start(), calls=%async_computation.13 | async-start | bytes 1310720 | tf_op jit(solution)/shard_map/all_gather | solution.py:147
  32.7 126.7 %all-gather.15.cloned.1.call-start = ((), (), s32[]{:S(2)}) async-start(), calls=%async_computation.11 | async-start | bytes 1310720 | tf_op jit(solution)/shard_map/all_gather | solution.py:148
  42.8 8.8 %all-to-all-start = ((bf16[256,4,128]{0,2,1:T(8,128)(2,1)}), bf16[256,4,128]{0,2,1:T(8,128)(2,1)S(1)}, u32[]{:S(2)}, u32[]{:S(2)}) async-start(bf16[256,4,128]{0,2,1:T(8,128)(2,1)} %bitcast.2), calls=%async_computation | async-start | bytes 524288 | tf_op jit(solution)/shard_map/all_to_all | solution.py:139
  46.2 155.7 %all-gather.13.cloned.1.call-start = ((), (), s32[]{:S(2)}) async-start(), calls=%async_computation.10 | async-start | bytes 1310720 | tf_op jit(solution)/shard_map/all_gather | solution.py:145
  105.5 29.6 %all-to-all-start.5 = ((bf16[4,128,128]{1,2,0:T(8,128)(2,1)}), bf16[4,128,128]{1,2,0:T(8,128)(2,1)S(1)}, u32[]{:S(2)}, u32[]{:S(2)}) async-start(bf16[4,128,128]{1,2,0:T(8,128)(2,1)} %copy.60), calls=%async_computation.5 | async-start | bytes 262144 | tf_op jit(solution)/shard_map/all_to_all | solution.py:156
  135.1 28.7 %all-to-all-start.7 = ((bf16[4,128,128]{1,2,0:T(8,128)(2,1)}), bf16[4,128,128]{1,2,0:T(8,128)(2,1)S(1)}, u32[]{:S(2)}, u32[]{:S(2)}) async-start(bf16[4,128,128]{1,2,0:T(8,128)(2,1)} %copy.65), calls=%async_computation.7 | async-start | bytes 262144 | tf_op jit(solution)/shard_map/all_to_all | solution.py:156
  163.8 22.6 %copy-start.7 = (f32[1024]{0:T(1024)S(1)}, f32[1024]{0:T(1024)}, u32[]{:S(2)}) copy-start(f32[1024]{0:T(1024)} %param.24) | copy-start | bytes 12292
  163.8 22.7 %copy-start.6 = (s32[4]{0:T(128)S(1)}, s32[4]{0:T(128)}, u32[]{:S(2)}) copy-start(s32[4]{0:T(128)} %constant.99.clone) | copy-start | bytes 52
  163.8 23.4 %copy-start.4 = (f32[1,2,64,256]{3,2,1,0:T(8,128)S(1)}, f32[1,2,64,256]{3,2,1,0:T(8,128)}, u32[]{:S(2)}) copy-start(f32[1,2,64,256]{3,2,1,0:T(8,128)} %param.26) | copy-start | bytes 393220
  163.8 8.8 %all-to-all-start.3 = ((bf16[4,128,128]{2,1,0:T(8,128)(2,1)}), bf16[4,128,128]{2,1,0:T(8,128)(2,1)S(1)}, u32[]{:S(2)}, u32[]{:S(2)}) async-start(bf16[4,128,128]{2,1,0:T(8,128)(2,1)} %bitcast.22), calls=%async_computation.3 | async-start | bytes 262144 | tf_op jit(solution)/shard_map/all_to_all | solution.py:156
  167.6 69.0 %all-gather.25.cloned.1.call-start = ((), (), s32[]{:S(2)}) async-start(), calls=%async_computation.17 | async-start | bytes 2621440 | tf_op jit(solution)/shard_map/all_gather | solution.py:27
  174.2 151.0 %all-gather.21.cloned.1.call-start = ((), (), s32[]{:S(2)}) async-start(), calls=%async_computation.14 | async-start | bytes 4456448 | tf_op jit(solution)/shard_map/all_gather | solution.py:209
  174.9 238.0 %all-gather.23.cloned.1.call-start = ((), (), s32[]{:S(2)}) async-start(), calls=%async_computation.15 | async-start | bytes 4456448 | tf_op jit(solution)/shard_map/all_gather | solution.py:210
  206.4 8.3 %all-to-all-start.1 = ((bf16[4,128,128]{1,2,0:T(8,128)(2,1)}), bf16[4,128,128]{1,2,0:T(8,128)(2,1)S(1)}, u32[]{:S(2)}, u32[]{:S(2)}) async-start(bf16[4,128,128]{1,2,0:T(8,128)(2,1)} %copy.52), calls=%async_computation.1 | async-start | bytes 262144 | tf_op jit(solution)/shard_map/all_to_all | solution.py:156
  209.7 215.7 %reduce-scatter.2.cloned.1.call-start = ((), (), s32[]{:S(2)}) async-start(), calls=%async_computation.16 | async-start | bytes 1572864 | tf_op jit(solution)/shard_map/reduce_scatter | solution.py:214
  214.9 4.6 %collective-permute-start = (bf16[16,512]{1,0:T(8,128)(2,1)S(1)}, bf16[16,512]{1,0:T(8,128)(2,1)S(1)}, u32[]{:S(2)}, u32[]{:S(2)}) collective-permute-start(bf16[16,512]{1,0:T(8,128)(2,1)S(1)} %copy.75), channel_id=1, source_target_pairs={{0,8},{8,16},{16,24},{1,9},{9,17},{17,25},{2,10},{10,18},{18,26},{... | collective-permute-start | bytes 49160 | tf_op jit(solution)/shard_map/ppermute | solution.py:22
Sparse Core Ops, SparseCore 0:
  19.4 27.6 all-gather.16
  49.0 51.9 all-gather.10
  102.6 27.9 all-gather.18
  132.0 27.3 all-gather.14
  160.8 28.7 all-gather.12
  191.1 45.4 all-gather.24
  239.3 85.8 all-gather.20
  327.9 84.9 all-gather.22
  418.9 6.5 reduce-scatter.1
where the time goes:
time: 433 us; the launch traced here: 432 us
  waiting for transfers between devices  297 us (69%)
  blocking collectives  52.3 us (12%)
  matrix products  25.7 us (6%)
  starting transfers between devices  20.9 us (5%)
  between operations  14.2 us (3%)
  other arithmetic  11.1 us (3%)
  local copies, waits for them, and re-layouts  10.4 us (2%)
    all_gather x1, waiting for transfers between devices, on_device(): lax.all_gather(retention_back, ('sp', 'fs'), axis=1, tiled=True)  87.7 us
    all_gather x1, waiting for transfers between devices, on_device(): lax.all_gather(pool_back, ('sp', 'fs'), axis=1, tiled=True)  83.7 us
    all_gather x1, waiting for transfers between devices, on_device(): group_normed = lax.all_gather(normed, 'fs', axis=0, tiled=True)  48.6 us
    all_gather x1, waiting for transfers between devices, on_device(): lax.all_gather(quarters[2], 'sp', axis=0, tiled=True)  21.8 us
    all_gather x1, waiting for transfers between devices, on_device(): lax.all_gather(quarters[3], 'sp', axis=0, tiled=True)  20.7 us
    dot_general x4, matrix products, on_device(): jnp.dot(group_normed, piece_w, preferred_element_type=jnp.float32)  15.6 us
    all_gather x1, waiting for transfers between devices, carried_in(): pieces = jax.tree.map(lambda part: lax.all_gather(part, axis), value)  14.9 us
    all_gather x1, blocking collectives, on_device(): whole_start = lax.all_gather(start_state, 'sp', axis=2, tiled=True)[0]  14.7 us
  transfers between devices with their start and end apart: 15, of which 11 were waited for; matrix products, arithmetic and copies ran while one was open for 9% of the time, Pallas kernels for 0%

commit v1 on v0

--- a/solution.py
+++ b/solution.py
@@ -134,7 +134,12 @@
     normed = (
         floats * lax.rsqrt(jnp.mean(floats * floats, axis=-1, keepdims=True) + eps) * norm_gain
     ).astype(jnp.bfloat16)
-    group_normed = lax.all_gather(normed, "fs", axis=0, tiled=True)
+    ring = [normed]
+    for hop in range(3):
+        ring.append(lax.ppermute(ring[-1], "fs", [(dev, (dev + 1) % 4) for dev in range(4)]))
+    group_normed = jnp.roll(
+        jnp.concatenate(ring[::-1], axis=0), (lax.axis_index("fs") + 1) * ring[0].shape[0], axis=0
+    )
     quarters = (
         lax.all_to_all(pool_proj, "fs", split_axis=1, concat_axis=0, tiled=True),
         lax.all_to_all(query_proj, "fs", split_axis=1, concat_axis=0, tiled=True),

time: 433 us -> 411 us (0.949)
  waiting for transfers between devices: 297 us -> 235 us
  blocking collectives: 52.3 us -> 67.8 us
  local copies, waits for them, and re-layouts: 10.4 us -> 24.5 us
  starting transfers between devices: 20.9 us -> 27.9 us
    all_gather x1 -> x0, waiting for transfers between devices: 48.6 us -> none  [on_device(): group_normed = lax.all_gather(normed, 'fs', axis=0, tiled=True)]
    ppermute x0 -> x3, waiting for transfers between devices: none -> 43.5 us  [on_device(): lax.ppermute(ring[-1], 'fs', [(dev, (dev + 1) % 4) for dev in range(4)])]
    all_gather x1, waiting for transfers between devices: 21.8 us -> 0.01 us  [on_device(): lax.all_gather(quarters[2], 'sp', axis=0, tiled=True)]
    all_gather x1, waiting for transfers between devices: 20.7 us -> 0.01 us  [on_device(): lax.all_gather(quarters[3], 'sp', axis=0, tiled=True)]
    all_to_all x1, blocking collectives: 8.11 us -> 24.4 us  [on_device(): lax.all_to_all(value_proj, 'fs', split_axis=1, concat_axis=0, tiled=True)]
    all_gather x1, waiting for transfers between devices: 14.9 us -> 0.02 us  [carried_in(): pieces = jax.tree.map(lambda part: lax.all_gather(part, axis), value)]
    unnamed x28 -> x34, local copies, waits for them, and re-layouts: 3.29 us -> 17.4 us
    all_to_all x1 -> x0, blocking collectives: 10.7 us -> none  [on_device(): lax.all_to_all(query_proj, 'fs', split_axis=1, concat_axis=0, tiled=True)]
  transfers between devices with their start and end apart: 15 -> 18, of which waited for: 11 -> 10; matrix products, arithmetic and copies ran while one was open for 9% -> 14% of each run, Pallas kernels for 0% -> 0%
where the time goes in v1:
time: 411 us; the launch traced here: 410 us
  waiting for transfers between devices  235 us (57%)
  blocking collectives  67.8 us (16%)
  starting transfers between devices  27.9 us (7%)
  matrix products  25.9 us (6%)
  local copies, waits for them, and re-layouts  24.5 us (6%)
  between operations  14.6 us (4%)
  other arithmetic  13.7 us (3%)
    all_gather x1, waiting for transfers between devices, on_device(): lax.all_gather(retention_back, ('sp', 'fs'), axis=1, tiled=True)  87.7 us
    all_gather x1, waiting for transfers between devices, on_device(): lax.all_gather(pool_back, ('sp', 'fs'), axis=1, tiled=True)  84.3 us
    ppermute x3, waiting for transfers between devices, on_device(): lax.ppermute(ring[-1], 'fs', [(dev, (dev + 1) % 4) for dev in range(4)])  43.5 us
    all_to_all x1, blocking collectives, on_device(): lax.all_to_all(value_proj, 'fs', split_axis=1, concat_axis=0, tiled=True)  24.4 us
    all_gather x1, blocking collectives, on_device(): whole_start = lax.all_gather(start_state, 'sp', axis=2, tiled=True)[0]  20.4 us
    unnamed x34, local copies, waits for them, and re-layouts  17.4 us
    dot_general x4, matrix products, on_device(): jnp.dot(group_normed, piece_w, preferred_element_type=jnp.float32)  15.6 us
    all_to_all x4, starting transfers between devices, on_device(): lax.all_to_all(shortened(rounded), 'fs', split_axis=0, concat_axis=1, til...  14 us
  transfers between devices with their start and end apart: 18, of which 10 were waited for; matrix products, arithmetic and copies ran while one was open for 14% of the time, Pallas kernels for 0%

profile of v1, /device:TPU:0, one launch (start us, length us, event | category | flops | bytes accessed | tf_op | source)
XLA Modules:
  0.0 409.7 jit_solution(10076306126153238768)
XLA Ops:
  6.6 1.2 copy.63
  7.8 10.8 %all_to_all.137 = bf16[256,4,128]{0,2,1:T(8,128)(2,1)S(1)} all-to-all(bf16[256,4,128]{0,2,1:T(8,128)(2,1)S(1)} %bitcast.100), channel_id=1, replica_groups=mesh['sp'=4,'fs'=4,'tp'=2] {'fs'}, dimensions={1} | all-to-all | bytes 524288 | tf_op jit(solution)/shard_map/all_to_all | solution.py:146
  18.6 0.8 copy.64
  19.5 1.8 copy.58
  21.3 3.4 all-to-all-start.4
  24.8 1.6 fusion.16
  26.3 2.6 fusion.18
  28.9 1.9 collective-permute-start
  30.8 0.8 copy.59
  31.8 21.8 %collective-permute-done = bf16[128,4096]{1,0:T(8,128)(2,1)S(1)} collective-permute-done((bf16[128,4096]{1,0:T(8,128)(2,1)}, bf16[128,4096]{1,0:T(8,128)(2,1)S(1)}, u32[]{:S(2)}, u32[]{:S(2)}) %collective-permute-start) | collective-permute-done | bytes 1048608 | tf_op jit(solution)/shard_map/ppermute | solution.py:139
  53.5 0.8 collective-permute-start.1
  54.4 1.1 copy.55
  55.5 24.4 %all_to_all.138 = bf16[256,4,128]{0,2,1:T(8,128)(2,1)S(1)} all-to-all(bf16[256,4,128]{0,2,1:T(8,128)(2,1)S(1)} %bitcast.101), channel_id=1, replica_groups=mesh['sp'=4,'fs'=4,'tp'=2] {'fs'}, dimensions={1} | all-to-all | bytes 524288 | tf_op jit(solution)/shard_map/all_to_all | solution.py:147
  79.9 0.8 copy.56
  80.8 0.8 copy.50
  81.6 3.4 all-to-all-start
  85.1 1.9 collective-permute-start.2
  87.0 0.7 dynamic-slice.2
  89.0 2.6 all-to-all-done
  91.6 0.8 copy.51
  92.4 21.7 %collective-permute-done.2 = bf16[128,4096]{1,0:T(8,128)(2,1)} collective-permute-done((bf16[128,4096]{1,0:T(8,128)(2,1)}, bf16[128,4096]{1,0:T(8,128)(2,1)}, u32[]{:S(2)}, u32[]{:S(2)}) %collective-permute-start.2) | collective-permute-done | bytes 1048608 | tf_op jit(solution)/shard_map/ppermute | solution.py:139
  114.1 2.3 constant_dynamic-update-slice_fusion.7
  116.4 2.4 constant_dynamic-update-slice_fusion.6
  118.8 1.0 constant_dynamic-update-slice_fusion.5
  119.8 1.3 constant_dynamic-update-slice_fusion.4
  121.1 2.3 constant_dynamic-update-slice_fusion.3
  123.4 2.3 constant_dynamic-update-slice_fusion.2
  125.8 1.1 constant_dynamic-update-slice_fusion.1
  126.8 1.4 constant_dynamic-update-slice_fusion
  128.2 3.8 fusion.29
  132.0 0.8 copy.65
  132.7 3.3 all-to-all-start.7
  136.1 3.8 fusion.26
  139.9 0.8 copy.60
  140.7 0.4 all-to-all-done.7
  141.0 3.8 all-to-all-start.5
  144.8 4.4 %fusion.23 = bf16[512,128]{1,0:T(8,128)(2,1)} fusion(bf16[4096,128]{1,0:T(8,128)(2,1)} %all-gather.12.cloned.1.call-done, bf16[1024,4096]{1,0:T(8,128)(2,1)} %constant_dynamic-update-slice_fusion, s32[]{:T(128)S(6)} %select_n.53), kind=kOutput, calls=%fused_computation.26 | convolution fusion | flops 536936448 | bytes 5373956 | tf_op jit(solution)/shard_map/dot_general | solution.py:156
  149.2 0.6 all-to-all-done.5
  149.8 3.6 all-to-all-start.3
  153.9 4.5 %all-to-all-done.3 = bf16[4,128,128]{2,1,0:T(8,128)(2,1)S(1)} async-done(((bf16[4,128,128]{2,1,0:T(8,128)(2,1)}), bf16[4,128,128]{2,1,0:T(8,128)(2,1)S(1)}, u32[]{:S(2)}, u32[]{:S(2)}) %all-to-all-start.3) | async-done | bytes 131104 | tf_op jit(solution)/shard_map/all_to_all | solution.py:161
  158.7 1.3 convolution_add_fusion
  160.0 0.5 all-gather.18.cloned.1.call-update
  160.6 0.7 all-gather.20.cloned.1.call-update
  161.3 12.1 %all-reduce = f32[8]{0:T(128)S(1)} all-reduce(f32[8]{0:T(128)S(1)} %get-tuple-element.181), channel_id=2, replica_groups=mesh['sp'=4,'fs'=4,'tp'=2] {'sp'}, use_global_device_ids=true, to_apply=%add | all-reduce | flops 8 | bytes 64
  173.6 0.6 fusion.77
  174.3 20.4 %all_gather.41 = f32[1,2,256,256]{3,2,1,0:T(8,128)S(1)} all-gather(f32[1,2,64,256]{3,2,1,0:T(8,128)S(1)} %copy-done.4), channel_id=1, replica_groups=mesh['sp'=4,'fs'=4,'tp'=2] {'sp'}, dimensions={2}, use_global_device_ids=true | all-gather | bytes 655360 | tf_op jit(solution)/shard_map/all_gather | solution.py:198
  194.7 3.7 fusion.20
  198.4 0.8 copy.52
  199.2 3.3 all-to-all-start.1
  202.5 1.2 minimum_convert_fusion
  203.7 3.7 all-to-all-done.1
  207.7 2.1 collective-permute-start.3
  209.8 0.4 convolution_multiply_fusion
  210.5 0.7 convolution_add_fusion.2
  211.4 1.1 fusion.34
  213.3 3.6 while.9
  213.4 1.2 fusion.87
  214.6 1.2 fusion.87
  215.8 1.2 fusion.87
  217.0 1.2 multiply_reduce_fusion
  218.3 84.3 %all-gather.18.cloned.1.call-done = bf16[512,4096]{1,0:T(8,128)(2,1)} async-done(((bf16[512,256]{1,0:T(8,128)(2,1)}), bf16[512,4096]{1,0:T(8,128)(2,1)}) %all-gather.18.cloned.1.call-update) | async-done | bytes 4194320 | tf_op jit(solution)/shard_map/all_gather | solution.py:214
  302.6 87.7 %all-gather.20.cloned.1.call-done = bf16[512,4096]{1,0:T(8,128)(2,1)} async-done(((bf16[512,256]{1,0:T(8,128)(2,1)}), bf16[512,4096]{1,0:T(8,128)(2,1)}) %all-gather.20.cloned.1.call-update) | async-done | bytes 4194320 | tf_op jit(solution)/shard_map/all_gather | solution.py:215
  390.3 5.9 %fusion.5 = bf16[128,4096]{1,0:T(8,128)(2,1)} fusion(bf16[512,4096]{1,0:T(8,128)(2,1)} %all-gather.20.cloned.1.call-done, bf16[512,4096]{1,0:T(8,128)(2,1)} %all-gather.18.cloned.1.call-done, bf16[128,512]{1,0:T(8,128)(2,1)S(1)} %copy.76, bf16[128,512]{1,0:T(8,128)(2,1)S(1)} %fusion.35), kind=kOutput, calls=%fused_computation.7 | convolution fusion | flops 1091567616 | bytes 9699328 | tf_op jit(solution)/shard_map/dot_general | solution.py:220
  396.2 6.7 %reduce-scatter.2.cloned.1.call-done = bf16[64,4096]{1,0:T(8,128)(2,1)} async-done(((bf16[128,4096]{1,0:T(8,128)(2,1)}), bf16[64,4096]{1,0:T(8,128)(2,1)}) %reduce-scatter.2.cloned.1.call-update) | async-done | bytes 524304 | tf_op jit(solution)/shard_map/reduce_scatter | solution.py:219
  (80 shorter events, 3.6 us)
Async XLA Ops:
  6.5 206.2 %copy-start = (bf16[4,256,256]{2,1,0:T(8,128)(2,1)S(1)}, bf16[4,256,256]{2,1,0:T(8,128)(2,1)}, u32[]{:S(2)}) copy-start(bf16[4,256,256]{2,1,0:T(8,128)(2,1)} %param.23) | copy-start | bytes 1572868
  6.5 80.5 %copy-start.8 = (u32[32]{0:T(128)S(1)}, u32[32]{0:T(128)}, u32[]{:S(2)}) copy-start(u32[32]{0:T(128)} %constant.126) | copy-start | bytes 388
  6.5 74.2 %copy-start.2 = (bf16[256,512]{1,0:T(8,128)(2,1)S(1)}, bf16[256,512]{1,0:T(8,128)(2,1)}, u32[]{:S(2)}) copy-start(bf16[256,512]{1,0:T(8,128)(2,1)} %param.19) | copy-start | bytes 786436
  6.5 82.0 %copy-start.5 = (f32[2]{0:T(128)S(1)}, f32[2]{0:T(128)}, u32[]{:S(2)}) copy-start(f32[2]{0:T(128)} %param.25) | copy-start | bytes 28
  6.5 121.7 %all-gather.16.cloned.1.call-start = ((), (), s32[]{:S(2)}) async-start(), calls=%async_computation.12 | async-start | bytes 1310720 | tf_op jit(solution)/shard_map/all_gather | solution.py:152
  7.8 112.1 %copy-start.1 = (bf16[1,128,4096]{2,1,0:T(8,128)(2,1)S(1)}, bf16[1,128,4096]{2,1,0:T(8,128)(2,1)}, u32[]{:S(2)}) copy-start(bf16[1,128,4096]{2,1,0:T(8,128)(2,1)} %param.17) | copy-start | bytes 3145732
  7.8 112.0 %copy-start.3 = (f32[4096]{0:T(1024)S(1)}, f32[4096]{0:T(1024)}, u32[]{:S(2)}) copy-start(f32[4096]{0:T(1024)} %param.18) | copy-start | bytes 49156
  21.3 9.5 %all-to-all-start.4 = ((bf16[256,4,128]{0,2,1:T(8,128)(2,1)}), bf16[256,4,128]{0,2,1:T(8,128)(2,1)S(1)}, u32[]{:S(2)}, u32[]{:S(2)}) async-start(bf16[256,4,128]{0,2,1:T(8,128)(2,1)} %bitcast.25), calls=%async_computation.4 | async-start | bytes 524288 | tf_op jit(solution)/shard_map/all_to_all | solution.py:145
  24.7 111.4 %all-gather.14.cloned.1.call-start = ((), (), s32[]{:S(2)}) async-start(), calls=%async_computation.11 | async-start | bytes 1310720 | tf_op jit(solution)/shard_map/all_gather | solution.py:151
  28.9 24.6 %collective-permute-start = (bf16[128,4096]{1,0:T(8,128)(2,1)}, bf16[128,4096]{1,0:T(8,128)(2,1)S(1)}, u32[]{:S(2)}, u32[]{:S(2)}) collective-permute-start(bf16[128,4096]{1,0:T(8,128)(2,1)} %fusion.18), channel_id=1, source_target_pairs={{0,2},{2,4},{4,6},{6,0},{1,3},{3,5},{5,7},{7,1},{8,10},{10,12},{12... | collective-permute-start | bytes 3145736 | tf_op jit(solution)/shard_map/ppermute | solution.py:139
  31.7 113.1 %all-gather.12.cloned.1.call-start = ((), (), s32[]{:S(2)}) async-start(), calls=%async_computation.10 | async-start | bytes 1310720 | tf_op jit(solution)/shard_map/all_gather | solution.py:153
  53.5 31.6 %collective-permute-start.1 = (bf16[128,4096]{1,0:T(8,128)(2,1)S(1)}, bf16[128,4096]{1,0:T(8,128)(2,1)}, u32[]{:S(2)}, u32[]{:S(2)}) collective-permute-start(bf16[128,4096]{1,0:T(8,128)(2,1)S(1)} %collective-permute-done), channel_id=1, source_target_pairs={{0,2},{2,4},{4,6},{6,0},{1,3},{3,5},{5,7},{7,1},{8,10},{10,12},{12... | collective-permute-start | bytes 3145736 | tf_op jit(solution)/shard_map/ppermute | solution.py:139
  81.6 9.9 %all-to-all-start = ((bf16[256,4,128]{0,2,1:T(8,128)(2,1)}), bf16[256,4,128]{0,2,1:T(8,128)(2,1)S(1)}, u32[]{:S(2)}, u32[]{:S(2)}) async-start(bf16[256,4,128]{0,2,1:T(8,128)(2,1)} %bitcast.2), calls=%async_computation | async-start | bytes 524288 | tf_op jit(solution)/shard_map/all_to_all | solution.py:144
  85.0 109.6 %all-gather.10.cloned.1.call-start = ((), (), s32[]{:S(2)}) async-start(), calls=%async_computation.9 | async-start | bytes 1310720 | tf_op jit(solution)/shard_map/all_gather | solution.py:150
  85.1 29.0 %collective-permute-start.2 = (bf16[128,4096]{1,0:T(8,128)(2,1)}, bf16[128,4096]{1,0:T(8,128)(2,1)}, u32[]{:S(2)}, u32[]{:S(2)}) collective-permute-start(bf16[128,4096]{1,0:T(8,128)(2,1)} %collective-permute-done.1), channel_id=1, source_target_pairs={{0,2},{2,4},{4,6},{6,0},{1,3},{3,5},{5,7},{7,1},{8,10},{10,12},{12... | collective-permute-start | bytes 3145736 | tf_op jit(solution)/shard_map/ppermute | solution.py:139
  132.7 8.3 %all-to-all-start.7 = ((bf16[4,128,128]{1,2,0:T(8,128)(2,1)}), bf16[4,128,128]{1,2,0:T(8,128)(2,1)S(1)}, u32[]{:S(2)}, u32[]{:S(2)}) async-start(bf16[4,128,128]{1,2,0:T(8,128)(2,1)} %copy.65), calls=%async_computation.7 | async-start | bytes 262144 | tf_op jit(solution)/shard_map/all_to_all | solution.py:161
  136.1 37.5 %copy-start.7 = (f32[1024]{0:T(1024)S(1)}, f32[1024]{0:T(1024)}, u32[]{:S(2)}) copy-start(f32[1024]{0:T(1024)} %param.24) | copy-start | bytes 12292
  136.1 37.5 %copy-start.6 = (s32[4]{0:T(128)S(1)}, s32[4]{0:T(128)}, u32[]{:S(2)}) copy-start(s32[4]{0:T(128)} %constant.121.clone) | copy-start | bytes 52
  136.1 38.2 %copy-start.4 = (f32[1,2,64,256]{3,2,1,0:T(8,128)S(1)}, f32[1,2,64,256]{3,2,1,0:T(8,128)}, u32[]{:S(2)}) copy-start(f32[1,2,64,256]{3,2,1,0:T(8,128)} %param.26) | copy-start | bytes 393220
  141.0 8.8 %all-to-all-start.5 = ((bf16[4,128,128]{1,2,0:T(8,128)(2,1)}), bf16[4,128,128]{1,2,0:T(8,128)(2,1)S(1)}, u32[]{:S(2)}, u32[]{:S(2)}) async-start(bf16[4,128,128]{1,2,0:T(8,128)(2,1)} %copy.60), calls=%async_computation.5 | async-start | bytes 262144 | tf_op jit(solution)/shard_map/all_to_all | solution.py:161
  149.8 8.6 %all-to-all-start.3 = ((bf16[4,128,128]{2,1,0:T(8,128)(2,1)}), bf16[4,128,128]{2,1,0:T(8,128)(2,1)S(1)}, u32[]{:S(2)}, u32[]{:S(2)}) async-start(bf16[4,128,128]{2,1,0:T(8,128)(2,1)} %bitcast.22), calls=%async_computation.3 | async-start | bytes 262144 | tf_op jit(solution)/shard_map/all_to_all | solution.py:161
  153.5 59.9 %all-gather.22.cloned.1.call-start = ((), (), s32[]{:S(2)}) async-start(), calls=%async_computation.16 | async-start | bytes 2621440 | tf_op jit(solution)/shard_map/all_gather | solution.py:27
  160.0 142.6 %all-gather.18.cloned.1.call-start = ((), (), s32[]{:S(2)}) async-start(), calls=%async_computation.13 | async-start | bytes 4456448 | tf_op jit(solution)/shard_map/all_gather | solution.py:214
  160.6 229.7 %all-gather.20.cloned.1.call-start = ((), (), s32[]{:S(2)}) async-start(), calls=%async_computation.14 | async-start | bytes 4456448 | tf_op jit(solution)/shard_map/all_gather | solution.py:215
  199.2 8.3 %all-to-all-start.1 = ((bf16[4,128,128]{1,2,0:T(8,128)(2,1)}), bf16[4,128,128]{1,2,0:T(8,128)(2,1)S(1)}, u32[]{:S(2)}, u32[]{:S(2)}) async-start(bf16[4,128,128]{1,2,0:T(8,128)(2,1)} %copy.52), calls=%async_computation.1 | async-start | bytes 262144 | tf_op jit(solution)/shard_map/all_to_all | solution.py:161
  202.5 200.4 %reduce-scatter.2.cloned.1.call-start = ((), (), s32[]{:S(2)}) async-start(), calls=%async_computation.15 | async-start | bytes 1572864 | tf_op jit(solution)/shard_map/reduce_scatter | solution.py:219
  207.7 3.5 collective-permute-start.3
Sparse Core Ops, SparseCore 0:
  19.6 27.6 all-gather.15
  48.9 27.3 all-gather.13
  80.9 28.2 all-gather.11
  110.6 27.3 all-gather.9
  160.1 52.6 all-gather.21
  215.4 87.1 all-gather.17
  305.3 84.9 all-gather.19
  396.3 6.5 reduce-scatter.1
